TPU v7x, 32 devices: a whole 2x2x4 slice. The times are simulated.
32 devices in a mesh: rep: 2 (over x), fs: 4 (over y, core), tp: 4 (over z).
Axes of the slice: x: 2, y: 2, z: 4, core: 2. Of those that a mesh axis runs over, the one named last changes fastest.
Arguments:
- acts: bfloat16 [2048, 2048], P(('rep', 'fs'), 'tp'), may hold values from -6 to 6
- cotangent: bfloat16 [2048, 2048], P(('rep', 'fs'), 'tp'), may hold values from -8 to 8
- pre_act: bfloat16 [2048, 4096], P(('rep', 'fs'), 'tp'), may hold values from -6 to 6
- up_store: float32 [2048, 4096], P('fs', 'tp'), may hold values from -0.125 to 0.125
- up_scale: float32 [4096], P('tp'), may hold values from 0.5 to 2
- down_store: float32 [4096, 2048], P('tp', 'fs'), may hold values from -0.09375 to 0.09375
- down_scale: float32 [2048], replicated, may hold values from 0.5 to 2
Outputs:
- grad_input: bfloat16 [2048, 2048], P(('rep', 'fs'), 'tp')
- grad_up: float32 [2048, 4096], P('fs', 'tp')
- grad_down: float32 [4096, 2048], P('tp', 'fs')
All inputs are finite; a program needn't handle non-finite values.
Results may differ from a plain program's by a relative error of at most 0.007.
Values may be sent and summed in bfloat16 or wider, within the bound.
A program may use at most 128 MiB of HBM per device.

v0:
```python
import math

import jax
import jax.numpy as jnp
from jax import lax
from jax.sharding import PartitionSpec as P


def contract_last(left, right):
    return lax.dot_general(
        left, right, (((1,), (1,)), ((), ())), preferred_element_type=jnp.float32
    )


def contract_first(left, right):
    return lax.dot_general(
        left, right, (((0,), (0,)), ((), ())), preferred_element_type=jnp.float32
    )


def body(acts, cotangent, pre_act, up_store, up_scale, down_store, down_scale):
    tok_rows = acts.shape[0]
    norm_factor = 1.0 / math.sqrt(tok_rows * lax.axis_size("fs") * lax.axis_size("rep"))
    full_acts, full_cot = (
        lax.all_gather(acts, "tp", axis=1, tiled=True),
        lax.all_gather(cotangent, "tp", axis=1, tiled=True),
    )
    scaled = (full_cot.astype(jnp.float32) * down_scale[None, :]).astype(jnp.bfloat16)
    down_bf = down_store.astype(jnp.bfloat16)
    up_bf = up_store.astype(jnp.bfloat16)
    d_act = contract_last(scaled, lax.all_gather(down_bf, "fs", axis=1, tiled=True))
    positive = jnp.maximum(pre_act.astype(jnp.float32), 0.0)
    act = (positive * positive).astype(jnp.bfloat16)
    d_pre = (2.0 * positive * d_act * up_scale[None, :]).astype(jnp.bfloat16)
    acts_cols, scaled_cols = (
        lax.all_to_all(full_acts, "fs", split_axis=1, concat_axis=0, tiled=True),
        lax.all_to_all(scaled, "fs", split_axis=1, concat_axis=0, tiled=True),
    )
    act_group, dpre_group = (
        lax.all_gather(act, "fs", axis=0, tiled=True),
        lax.all_gather(d_pre, "fs", axis=0, tiled=True),
    )
    grad_down = contract_first(act_group, scaled_cols) * norm_factor
    grad_up = contract_first(acts_cols, dpre_group) * norm_factor
    partial_value = contract_last(d_pre, lax.all_gather(up_bf, "fs", axis=0, tiled=True))
    grad_input = lax.psum_scatter(partial_value, "tp", scatter_dimension=1, tiled=True).astype(
        jnp.bfloat16
    )
    grad_up, grad_down = lax.psum((grad_up, grad_down), "rep")
    return (grad_input, grad_up, grad_down)


def solution(mesh):
    return jax.shard_map(
        body,
        mesh=mesh,
        in_specs=(
            P(("rep", "fs"), "tp"),
            P(("rep", "fs"), "tp"),
            P(("rep", "fs"), "tp"),
            P("fs", "tp"),
            P("tp"),
            P("tp", "fs"),
            P(),
        ),
        out_specs=(P(("rep", "fs"), "tp"), P("fs", "tp"), P("tp", "fs")),
        check_vma=False,
    )
```

profile of v0, /device:TPU:5, one launch (start us, length us, event | category | flops | bytes accessed | tf_op | source)
XLA Modules:
  0.0 363.1 jit_solution(4651438372138626492)
XLA Ops:
  7.2 0.0 all-gather.7.cloned.1.call-start
  7.2 1.8 copy.12
  9.0 0.0 all-gather.7.cloned.1.call-update
  9.0 0.0 copy-start
  9.0 0.0 all-gather.9.cloned.1.call-start
  9.1 2.8 convert_element_type.27
  11.9 0.0 all-gather.9.cloned.1.call-update
  11.9 0.0 copy-start.3
  12.0 0.0 copy-start.2
  12.0 0.0 all-gather.11.cloned.1.call-start
  12.0 0.0 copy-done
  12.0 1.2 convert_element_type.29
  13.2 0.0 all-gather.11.cloned.1.call-update
  13.2 0.0 all-gather.15.cloned.1.call-start
  13.3 0.0 copy-done.3
  13.3 0.8 copy.13
  14.1 0.0 all-gather.15.cloned.1.call-update
  14.2 0.0 all-gather.17.cloned.1.call-start
  14.2 0.9 multiply_convert_fusion.1
  15.1 0.0 all-gather.17.cloned.1.call-update
  15.2 0.0 all-gather.13.cloned.1.call-start
  15.2 23.6 %all-gather.7.cloned.1.call-done = bf16[256,2048]{0,1:T(8,128)(2,1)} async-done(((bf16[256,512]{0,1:T(8,128)(2,1)}), bf16[256,2048]{0,1:T(8,128)(2,1)}) %all-gather.7.cloned.1.call-update) | async-done | bytes 1048592 | tf_op jit(solution)/shard_map/all_gather | solution.py:26
  38.9 2.5 multiply_convert_fusion
  41.4 33.2 %all-gather.9.cloned.1.call-done = bf16[1024,2048]{1,0:T(8,128)(2,1)} async-done(((bf16[1024,512]{1,0:T(8,128)(2,1)}), bf16[1024,2048]{1,0:T(8,128)(2,1)}) %all-gather.9.cloned.1.call-update) | async-done | bytes 4194320 | tf_op jit(solution)/shard_map/all_gather | solution.py:31
  74.6 4.7 %fusion.1 = bf16[256,1024]{1,0:T(8,128)(2,1)} fusion(bf16[256,2048]{0,1:T(8,128)(2,1)} %multiply_convert_fusion, bf16[1024,2048]{1,0:T(8,128)(2,1)} %all-gather.9.cloned.1.call-done, bf16[256,1024]{1,0:T(8,128)(2,1)S(1)} %copy-done.2, f32[1024]{0:T(1024)S(1)} %copy-done.5), kind=kOutput, calls=%fused_computation.5 | convolution fusion | flops 1075314688 | bytes 6295552 | tf_op jit(solution)/shard_map/dot_general | solution.py:10
  79.3 0.0 all-gather.13.cloned.1.call-update
  79.4 0.0 reduce-scatter.2.cloned.1.call-start
  79.4 31.2 %all-gather.11.cloned.1.call-done = bf16[2048,1024]{1,0:T(8,128)(2,1)} async-done(((bf16[512,1024]{1,0:T(8,128)(2,1)}), bf16[2048,1024]{1,0:T(8,128)(2,1)}) %all-gather.11.cloned.1.call-update) | async-done | bytes 4194320 | tf_op jit(solution)/shard_map/all_gather | solution.py:45
  110.7 5.0 %fusion.2 = f32[256,2048]{1,0:T(8,128)} fusion(bf16[256,1024]{1,0:T(8,128)(2,1)} %fusion.1, bf16[2048,1024]{1,0:T(8,128)(2,1)} %all-gather.11.cloned.1.call-done), kind=kOutput, calls=%fused_computation.8 | convolution fusion | flops 1073741824 | bytes 6815744 | tf_op jit(solution)/shard_map/dot_general | solution.py:10
  115.6 0.0 reduce-scatter.2.cloned.1.call-update
  115.7 24.7 %all-gather.15.cloned.1.call-done = bf16[256,2048]{0,1:T(8,128)(2,1)} async-done(((bf16[256,512]{0,1:T(8,128)(2,1)}), bf16[256,2048]{0,1:T(8,128)(2,1)}) %all-gather.15.cloned.1.call-update) | async-done | bytes 1048592 | tf_op jit(solution)/shard_map/all_gather | solution.py:25
  140.4 24.6 %all_to_all.38 = bf16[256,4,512]{0,2,1:T(8,128)(2,1)S(1)} all-to-all(bf16[256,4,512]{0,2,1:T(8,128)(2,1)} %bitcast.18), channel_id=1, replica_groups=mesh['rep'=2,'fs'=4,'tp'=4] {'fs'}, dimensions={1} | all-to-all | bytes 2097152 | tf_op jit(solution)/shard_map/all_to_all | solution.py:36
  165.0 5.9 %all-to-all-start.1 = ((bf16[256,4,512]{0,2,1:T(8,128)(2,1)}), bf16[256,4,512]{0,2,1:T(8,128)(2,1)S(1)}, u32[]{:S(2)}, u32[]{:S(2)}) async-start(bf16[256,4,512]{0,2,1:T(8,128)(2,1)} %bitcast.4), calls=%async_computation.2 | async-start | bytes 2097152 | tf_op jit(solution)/shard_map/all_to_all | solution.py:37
  170.9 0.0 all-reduce.3.cloned.1.call-start
  170.9 0.5 copy.14
  171.4 15.3 %all-to-all-done.1 = bf16[256,4,512]{0,2,1:T(8,128)(2,1)S(1)} async-done(((bf16[256,4,512]{0,2,1:T(8,128)(2,1)}), bf16[256,4,512]{0,2,1:T(8,128)(2,1)S(1)}, u32[]{:S(2)}, u32[]{:S(2)}) %all-to-all-start.1) | async-done | bytes 1048608 | tf_op jit(solution)/shard_map/all_to_all | solution.py:37
  186.7 0.5 copy.15
  187.2 0.0 all-gather.17.cloned.1.call-done
  187.2 4.3 %convolution_multiply_fusion = f32[1024,512]{1,0:T(8,128)} fusion(bf16[1024,1024]{1,0:T(8,128)(2,1)} %all-gather.17.cloned.1.call-done, bf16[1024,512]{1,0:T(8,128)(2,1)S(1)} %bitcast.20), kind=kOutput, calls=%fused_computation.2 | convolution fusion | flops 1074266112 | bytes 5242880 | tf_op jit(solution)/shard_map/dot_general | solution.py:16
  191.5 5.0 %all-gather.13.cloned.1.call-done = bf16[1024,1024]{1,0:T(8,128)(2,1)} async-done(((bf16[256,1024]{1,0:T(8,128)(2,1)}), bf16[1024,1024]{1,0:T(8,128)(2,1)}) %all-gather.13.cloned.1.call-update) | async-done | bytes 2097168 | tf_op jit(solution)/shard_map/all_gather | solution.py:41
  196.6 4.2 %multiply_bitcast_fusion = f32[512,1024]{0,1:T(8,128)} fusion(bf16[1024,1024]{1,0:T(8,128)(2,1)} %all-gather.13.cloned.1.call-done, bf16[1024,512]{1,0:T(8,128)(2,1)S(1)} %bitcast.19), kind=kOutput, calls=%fused_computation | convolution fusion | flops 1074266112 | bytes 5242880 | tf_op jit(solution)/shard_map/dot_general | solution.py:16
  200.8 0.0 all-reduce.3.cloned.1.call-update
  200.8 40.7 %reduce-scatter.2.cloned.1.call-done = f32[256,512]{1,0:T(8,128)} async-done(((f32[256,2048]{1,0:T(8,128)}), f32[256,512]{1,0:T(8,128)}) %reduce-scatter.2.cloned.1.call-update) | async-done | bytes 524304 | tf_op jit(solution)/shard_map/reduce_scatter | solution.py:46
  241.5 1.8 convert_element_type.30
  243.2 108.7 %all-reduce.3.cloned.1.call-done = (f32[512,1024]{0,1:T(8,128)}, f32[1024,512]{1,0:T(8,128)}) async-done(((f32[512,1024]{0,1:T(8,128)}, f32[1024,512]{1,0:T(8,128)}), (f32[512,1024]{0,1:T(8,128)}, f32[1024,512]{1,0:T(8,128)})) %all-reduce.3.cloned.1.call-update) | async-done | bytes 4194320 | tf_op jit(solution)/shard_map/psum | solution.py:49
  351.9 3.0 copy.16
  354.9 0.0 copy-done.1
  354.9 1.3 copy.19
  (6 shorter events, 0.0 us)
Async XLA Ops:
  7.2 31.7 %all-gather.7.cloned.1.call-start = ((), (), s32[]{:S(2)}) async-start(), calls=%async_computation.3 | async-start | bytes 1310720 | tf_op jit(solution)/shard_map/all_gather | solution.py:26
  9.0 3.0 copy-start
  9.0 65.6 %all-gather.9.cloned.1.call-start = ((), (), s32[]{:S(2)}) async-start(), calls=%async_computation.4 | async-start | bytes 5242880 | tf_op jit(solution)/shard_map/all_gather | solution.py:31
  11.9 1.3 copy-start.3
  12.0 2.2 copy-start.2
  12.0 98.7 %all-gather.11.cloned.1.call-start = ((), (), s32[]{:S(2)}) async-start(), calls=%async_computation.5 | async-start | bytes 5242880 | tf_op jit(solution)/shard_map/all_gather | solution.py:45
  13.2 25.7 %copy-start.4 = (f32[2048]{0:T(1024)S(1)}, f32[2048]{0:T(1024)}, u32[]{:S(2)}) copy-start(f32[2048]{0:T(1024)} %param.13) | copy-start | bytes 24580
  13.2 127.1 %all-gather.15.cloned.1.call-start = ((), (), s32[]{:S(2)}) async-start(), calls=%async_computation.8 | async-start | bytes 1310720 | tf_op jit(solution)/shard_map/all_gather | solution.py:25
  14.1 60.5 %copy-start.5 = (f32[1024]{0:T(1024)S(1)}, f32[1024]{0:T(1024)}, u32[]{:S(2)}) copy-start(f32[1024]{0:T(1024)} %param.11) | copy-start | bytes 12292
  14.2 173.1 %all-gather.17.cloned.1.call-start = ((), (), s32[]{:S(2)}) async-start(), calls=%async_computation.9 | async-start | bytes 2621440 | tf_op jit(solution)/shard_map/all_gather | solution.py:40
  15.2 181.4 %all-gather.13.cloned.1.call-start = ((), (), s32[]{:S(2)}) async-start(), calls=%async_computation.7 | async-start | bytes 2621440 | tf_op jit(solution)/shard_map/all_gather | solution.py:41
  79.4 162.1 %reduce-scatter.2.cloned.1.call-start = ((), (), s32[]{:S(2)}) async-start(), calls=%async_computation.6 | async-start | bytes 2621440 | tf_op jit(solution)/shard_map/reduce_scatter | solution.py:46
  165.0 21.7 %all-to-all-start.1 = ((bf16[256,4,512]{0,2,1:T(8,128)(2,1)}), bf16[256,4,512]{0,2,1:T(8,128)(2,1)S(1)}, u32[]{:S(2)}, u32[]{:S(2)}) async-start(bf16[256,4,512]{0,2,1:T(8,128)(2,1)} %bitcast.4), calls=%async_computation.2 | async-start | bytes 2097152 | tf_op jit(solution)/shard_map/all_to_all | solution.py:37
  170.9 181.0 %all-reduce.3.cloned.1.call-start = ((), (), s32[]{:S(2)}) async-start(), calls=%async_computation.10 | async-start | bytes 8388608 | tf_op jit(solution)/shard_map/psum | solution.py:49
  351.9 3.0 copy-start.1
Sparse Core Ops, SparseCore 0:
  10.1 28.6 all-gather.6
  41.0 33.5 all-gather.8
  76.2 34.4 all-gather.10
  112.1 28.2 all-gather.14
  141.8 29.0 all-gather.16
  172.2 24.2 all-gather.12
  199.4 41.9 reduce-scatter.1
  244.5 107.3 all-reduce.2
where the time goes:
time: 365 us; the launch traced here: 363 us
  waiting for transfers between devices  283 us (78%)
  blocking collectives  24.6 us (7%)
  matrix products  18.2 us (5%)
  between operations  14.2 us (4%)
  other arithmetic  9.24 us (3%)
  local copies, waits for them, and re-layouts  8.08 us (2%)
  starting transfers between devices  6.22 us (2%)
    psum x1, waiting for transfers between devices, body(): grad_up, grad_down = lax.psum((grad_up, grad_down), 'rep')  109 us
    reduce_scatter x1, waiting for transfers between devices, body(): lax.psum_scatter(partial_value, 'tp', scatter_dimension=1, tiled=True)  40.7 us
    all_gather x1, waiting for transfers between devices, body(): lax.all_gather(down_bf, 'fs', axis=1, tiled=True)  33.2 us
    all_gather x1, waiting for transfers between devices, body(): lax.all_gather(up_bf, 'fs', axis=0, tiled=True)  31.2 us
    all_gather x1, waiting for transfers between devices, body(): lax.all_gather(acts, 'tp', axis=1, tiled=True)  24.7 us
    all_to_all x1, blocking collectives, body(): lax.all_to_all(full_acts, 'fs', split_axis=1, concat_axis=0, tiled=True)  24.6 us
    all_gather x1, waiting for transfers between devices, body(): lax.all_gather(cotangent, 'tp', axis=1, tiled=True)  23.6 us
    all_to_all x1, waiting for transfers between devices, body(): lax.all_to_all(scaled, 'fs', split_axis=1, concat_axis=0, tiled=True)  15.3 us
  transfers between devices with their start and end apart: 9, of which 8 were waited for; matrix products, arithmetic and copies ran while one was open for 8% of the time, Pallas kernels for 0%

commit v1 on v0

v1 whole, which is shorter than its diff:
```python
import functools
import math

import jax
import jax.numpy as jnp
from jax import lax
from jax.experimental import pallas as pl
from jax.experimental.pallas import tpu as pltpu
from jax.sharding import PartitionSpec as P

F32, BF16 = jnp.float32, jnp.bfloat16


def dot(left, right, dims):
    return lax.dot_general(left, right, (dims, ((), ())), preferred_element_type=F32)


def fitting(size, most):
    return most if size % most == 0 else size


def kernel(
    sizes,
    acts, cotangent, pre_act, up_store, up_scale, down_store, down_scale,
    grad_input, grad_up, grad_down,
    blocks, scaled_cols, acts_cols, act_group, dpre_group, down_bf, up_bf,
    pair_out, pair_in, far_out, far_in, d_act, gi_out, gi_in,
    gd_out, gd_in, gu_out, gu_in,
    z_send, z_recv, col_send, col_recv, act_send, act_recv, dpre_send, dpre_recv,
    pair_send, pair_recv, far_send, far_recv, gi_send, gi_recv,
    gd_send, gd_recv, gu_send, gu_recv,
):
    reps, F, T = sizes
    n, d = acts.shape
    h = pre_act.shape[1]
    w = down_store.shape[1]
    half, sub = F // 2, F // T
    norm_factor = 1.0 / math.sqrt(n * F * reps)
    r, f, z = lax.axis_index("rep"), lax.axis_index("fs"), lax.axis_index("tp")
    core, place = lax.rem(f, 2), lax.div(f, 2)
    partner = f + 1 - 2 * core

    def rows(at):
        return pl.ds(pl.multiple_of(at * n, n), n)

    def remote(src, dst, send, recv, where):
        return pltpu.make_async_remote_copy(
            src_ref=src, dst_ref=dst, send_sem=send, recv_sem=recv,
            device_id=where, device_id_type=pl.DeviceIdType.MESH,
        )

    def landed(ref, recv):
        remote(ref, ref, recv, recv, {"fs": partner}).wait_recv()

    def left_for(ref, send):
        remote(ref, ref, send, send, {"fs": partner}).wait_send()

    cols = (scaled_cols, acts_cols)

    def pass_on(a, block, way):
        @pl.when((z < T - 1) if way == 0 else (z > 0))
        def _():
            ref = blocks.at[a, block]
            to = z + 1 if way == 0 else z - 1
            remote(ref, ref, z_send.at[a, block, way], z_recv.at[a, block], {"tp": to}).start()

    def spread(a, block):
        for j in range(sub):
            target = block * sub + j

            @pl.when(target != f)
            def _():
                remote(
                    blocks.at[a, block, :, pl.ds(j * w, w)], cols[a].at[rows(f)],
                    col_send.at[a, target], col_recv.at[a, f], {"fs": target},
                ).start()

            @pl.when(target == f)
            def _():
                cols[a][rows(f), :] = blocks[a, block, :, j * w:(j + 1) * w]

    def own_block(a):
        pass_on(a, z, 0)
        pass_on(a, z, 1)
        spread(a, z)

    def arriving(a, s):
        @pl.when(z - s >= 0)
        def _():
            landed(blocks.at[a, z - s], z_recv.at[a, z - s])
            pass_on(a, z - s, 0)
            spread(a, z - s)

        @pl.when(z + s <= T - 1)
        def _():
            landed(blocks.at[a, z + s], z_recv.at[a, z + s])
            pass_on(a, z + s, 1)
            spread(a, z + s)

    def cols_landed(a, source):
        @pl.when(source != f)
        def _():
            landed(cols[a].at[rows(source)], col_recv.at[a, source])

    def group_start(group, send, recv):
        ref = group.at[rows(f)]
        for k in range(1, half):
            to = lax.rem(f + 2 * k, F)
            remote(ref, ref, send.at[k], recv.at[f], {"fs": to}).start()
        remote(ref, ref, send.at[0], recv.at[f], {"fs": partner}).start()

    def group_forward(group, send, recv, k):
        source = lax.rem(f - 2 * k + F, F)
        ref = group.at[rows(source)]
        landed(ref, recv.at[source])
        remote(ref, ref, send.at[half - 1 + k], recv.at[source], {"fs": partner}).start()
        return source

    def group_sent(group, send):
        for k in range(F - 1):
            left_for(group.at[rows(f)], send.at[k])

    scale = down_scale[:, pl.ds(pl.multiple_of(z * d, d), d)]
    blocks[0, z] = (cotangent[...].astype(F32) * scale).astype(BF16)
    own_block(0)
    positive = jnp.maximum(pre_act[...].astype(F32), 0.0)
    act_group[rows(f), :] = (positive * positive).astype(BF16)
    group_start(act_group, act_send, act_recv)
    blocks[1, z] = acts[...]
    down_bf[...] = down_store[...].astype(BF16)
    for s in range(1, T):
        arriving(0, s)
    own_block(1)
    up_bf[...] = up_store[...].astype(BF16)

    def partial_of(target):
        cols_landed(0, target)
        return dot(scaled_cols[rows(target), :], down_bf[...], ((1,), (1,)))

    def for_partner(k, carry):
        i = lax.rem(place + k, half)
        pair_out[i] = partial_of(2 * i + 1 - core).astype(BF16)
        remote(
            pair_out.at[i], pair_in.at[i], pair_send.at[i], pair_recv.at[i], {"fs": partner}
        ).start()
        return carry

    lax.fori_loop(1, half + 1, for_partner, 0)

    def for_far(k, carry):
        i = lax.rem(place + k, half)
        value = partial_of(2 * i + core)
        landed(pair_in.at[i], pair_recv.at[i])
        far_out[i] = (value + pair_in[i].astype(F32)).astype(BF16)
        remote(
            far_out.at[i], far_in.at[place], far_send.at[i], far_recv.at[place],
            {"fs": 2 * i + core},
        ).start()
        return carry

    lax.fori_loop(1, half, for_far, 0)
    value = partial_of(f)
    landed(pair_in.at[place], pair_recv.at[place])
    d_act[...] = value + pair_in[place].astype(F32)

    for k in range(1, half):
        group_forward(act_group, act_send, act_recv, k)
    for s in range(1, T):
        arriving(1, s)

    landed(act_group.at[rows(partner)], act_recv.at[partner])
    for k in range(1, half):
        source = lax.rem(partner + 2 * k, F)
        landed(act_group.at[rows(source)], act_recv.at[source])
    gd_rows = gd_out.shape[1]

    def rep_copy(out, into, send, recv, c, p):
        to = lax.rem(r + p, reps)
        return remote(
            out.at[c], into.at[p - 1, c], send.at[p - 1, c], recv.at[p - 1, c], {"rep": to}
        )

    def down_step(c, carry):
        at = pl.ds(pl.multiple_of(c * gd_rows, gd_rows), gd_rows)
        value = dot(act_group[:, at], scaled_cols[...], ((0,), (0,))) * norm_factor
        gd_out[c] = value.astype(BF16)
        for p in range(1, reps):
            rep_copy(gd_out, gd_in, gd_send, gd_recv, c, p).start()
        return carry

    lax.fori_loop(0, gd_out.shape[0], down_step, 0)

    total = d_act[...]
    for k in range(1, half):
        j = lax.rem(place + k, half)
        landed(far_in.at[j], far_recv.at[j])
        total = total + far_in[j].astype(F32)
    positive = jnp.maximum(pre_act[...].astype(F32), 0.0)
    dpre_group[rows(f), :] = (2.0 * positive * total * up_scale[...]).astype(BF16)
    group_start(dpre_group, dpre_send, dpre_recv)

    home = lax.div(f, sub)
    slot = z * sub + lax.rem(f, sub)

    def input_part(source):
        gi_out[source] = dot(dpre_group[rows(source), :], up_bf[...], ((1,), (1,))).astype(BF16)

        @pl.when((source != f) | (home != z))
        def _():
            remote(
                gi_out.at[source], gi_in.at[slot], gi_send.at[source], gi_recv.at[slot],
                {"fs": source, "tp": home},
            ).start()

        @pl.when((source == f) & (home == z))
        def _():
            gi_in[slot] = gi_out[source]

    input_part(f)
    for k in range(1, half):
        input_part(group_forward(dpre_group, dpre_send, dpre_recv, k))
    landed(dpre_group.at[rows(partner)], dpre_recv.at[partner])
    input_part(partner)
    for k in range(1, half):
        source = lax.rem(partner + 2 * k, F)
        landed(dpre_group.at[rows(source)], dpre_recv.at[source])
        input_part(source)

    for source in range(F):
        cols_landed(1, source)
    gu_rows = gu_out.shape[1]
    for c in range(gu_out.shape[0]):
        value = dot(acts_cols[:, c * gu_rows:(c + 1) * gu_rows], dpre_group[...], ((0,), (0,)))
        gu_out[c] = (value * norm_factor).astype(BF16)
        for p in range(1, reps):
            rep_copy(gu_out, gu_in, gu_send, gu_recv, c, p).start()

    def finish(out, into, send, recv, result):
        step_rows = out.shape[1]

        def step(c, carry):
            for p in range(1, reps):
                rep_copy(out, into, send, recv, c, p).wait()
            value = out[c].astype(F32)
            for p in range(1, reps):
                value = value + into[p - 1, c].astype(F32)
            result[pl.ds(pl.multiple_of(c * step_rows, step_rows), step_rows), :] = value
            return carry

        lax.fori_loop(0, out.shape[0], step, 0)

    finish(gd_out, gd_in, gd_send, gd_recv, grad_down)
    for j in range(sub):
        value = jnp.zeros((n, w), F32)
        for s in range(T):
            at = s * sub + j

            @pl.when((s != z) | (z * sub + j != f))
            def _():
                landed(gi_in.at[at], gi_recv.at[at])

            value = value + gi_in[at].astype(F32)
        grad_input[:, j * w:(j + 1) * w] = value.astype(BF16)
    finish(gu_out, gu_in, gu_send, gu_recv, grad_up)

    for a in range(2):
        for block in range(T):
            @pl.when((block <= z) & (z < T - 1))
            def _():
                left_for(blocks.at[a, block], z_send.at[a, block, 0])

            @pl.when((block >= z) & (z > 0))
            def _():
                left_for(blocks.at[a, block], z_send.at[a, block, 1])

        for target in range(F):
            @pl.when(target != f)
            def _():
                left_for(cols[a].at[rows(f)], col_send.at[a, target])
    group_sent(act_group, act_send)
    group_sent(dpre_group, dpre_send)
    for i in range(half):
        left_for(pair_out.at[i], pair_send.at[i])

        @pl.when(i != place)
        def _():
            left_for(far_out.at[i], far_send.at[i])
    for source in range(F):
        @pl.when((source != f) | (home != z))
        def _():
            left_for(gi_out.at[source], gi_send.at[source])


def body(sizes, acts, cotangent, pre_act, up_store, up_scale, down_store, down_scale):
    reps, F, T = sizes
    n, d = acts.shape
    h = pre_act.shape[1]
    w = down_store.shape[1]
    half, sub = F // 2, F // T
    gd_rows, gu_rows = fitting(h, 256), fitting(w, 256)
    gd_steps, gu_steps = h // gd_rows, w // gu_rows
    others = max(reps - 1, 1)
    sem = pltpu.SemaphoreType.DMA
    vmem = pl.BlockSpec(memory_space=pltpu.VMEM)
    return pl.pallas_call(
        functools.partial(kernel, sizes),
        out_shape=(
            jax.ShapeDtypeStruct((n, d), BF16),
            jax.ShapeDtypeStruct((w, h), F32),
            jax.ShapeDtypeStruct((h, w), F32),
        ),
        in_specs=[vmem] * 7,
        out_specs=(vmem, vmem, vmem),
        scratch_shapes=[
            pltpu.VMEM((2, T, n, d), BF16),
            pltpu.VMEM((F * n, w), BF16),
            pltpu.VMEM((F * n, w), BF16),
            pltpu.VMEM((F * n, h), BF16),
            pltpu.VMEM((F * n, h), BF16),
            pltpu.VMEM((h, w), BF16),
            pltpu.VMEM((w, h), BF16),
            pltpu.VMEM((half, n, h), BF16),
            pltpu.VMEM((half, n, h), BF16),
            pltpu.VMEM((half, n, h), BF16),
            pltpu.VMEM((half, n, h), BF16),
            pltpu.VMEM((n, h), F32),
            pltpu.VMEM((F, n, w), BF16),
            pltpu.VMEM((F, n, w), BF16),
            pltpu.VMEM((gd_steps, gd_rows, w), BF16),
            pltpu.VMEM((others, gd_steps, gd_rows, w), BF16),
            pltpu.VMEM((gu_steps, gu_rows, h), BF16),
            pltpu.VMEM((others, gu_steps, gu_rows, h), BF16),
            sem((2, T, 2)), sem((2, T)), sem((2, F)), sem((2, F)),
            sem((F,)), sem((F,)), sem((F,)), sem((F,)),
            sem((half,)), sem((half,)), sem((half,)), sem((half,)),
            sem((F,)), sem((F,)),
            sem((others, gd_steps)), sem((others, gd_steps)),
            sem((others, gu_steps)), sem((others, gu_steps)),
        ],
        compiler_params=pltpu.CompilerParams(
            has_side_effects=True, vmem_limit_bytes=60 * 1024 * 1024
        ),
    )(
        acts, cotangent, pre_act, up_store, up_scale.reshape(1, h), down_store,
        down_scale.reshape(1, d * T),
    )


def solution(mesh):
    sizes = (mesh.shape["rep"], mesh.shape["fs"], mesh.shape["tp"])
    return jax.shard_map(
        functools.partial(body, sizes),
        mesh=mesh,
        in_specs=(
            P(("rep", "fs"), "tp"),
            P(("rep", "fs"), "tp"),
            P(("rep", "fs"), "tp"),
            P("fs", "tp"),
            P("tp"),
            P("tp", "fs"),
            P(),
        ),
        out_specs=(P(("rep", "fs"), "tp"), P("fs", "tp"), P("tp", "fs")),
        check_vma=False,
    )
```

time: 365 us -> 118 us (0.32)
  waiting for transfers between devices: 283 us -> 0 us
  Pallas kernels: 0 us -> 110 us
  blocking collectives: 24.6 us -> 0 us
  matrix products: 18.2 us -> 0 us
  between operations: 14.2 us -> 0.64 us
  other arithmetic: 9.24 us -> 0 us
  starting transfers between devices: 6.22 us -> 0 us
    all_gather x6 -> x0, waiting for transfers between devices: 118 us -> none  [the longest x1 33.2 us: body(): lax.all_gather(down_bf, 'fs', axis=1, tiled=True)]
    pallas_call x0 -> x1, Pallas kernels: none -> 110 us  [body(): pl.pallas_call(functools.partial(kernel, sizes), out_shape=(jax.ShapeDtyp...]
    psum x1 -> x0, waiting for transfers between devices: 109 us -> none  [body(): grad_up, grad_down = lax.psum((grad_up, grad_down), 'rep')]
    reduce_scatter x1 -> x0, waiting for transfers between devices: 40.7 us -> none  [body(): lax.psum_scatter(partial_value, 'tp', scatter_dimension=1, tiled=True)]
    all_to_all x1 -> x0, blocking collectives: 24.6 us -> none  [body(): lax.all_to_all(full_acts, 'fs', split_axis=1, concat_axis=0, tiled=True)]
    dot_general x4 -> x0, matrix products: 18.2 us -> none  [the longest x2 9.69 us: contract_last(): lax.dot_general(left, right, (((1,), (1,)), ((), ())), preferred_element_...]
    all_to_all x1 -> x0, waiting for transfers between devices: 15.3 us -> none  [body(): lax.all_to_all(scaled, 'fs', split_axis=1, concat_axis=0, tiled=True)]
    convert_element_type x5 -> x0, other arithmetic: 9.24 us -> none  [the longest x1 2.83 us: body(): down_bf = down_store.astype(jnp.bfloat16)]
  transfers between devices with their start and end apart: 9 -> 0, of which waited for: 8 -> 0; matrix products, arithmetic and copies ran while one was open for 8% -> 0% of each run, Pallas kernels for 0% -> 0%
where the time goes in v1:
time: 118 us; the launch traced here: 117 us
  Pallas kernels  110 us (93%)
  local copies, waits for them, and re-layouts  6.3 us (5%)
    pallas_call x1, Pallas kernels, body(): pl.pallas_call(functools.partial(kernel, sizes), out_shape=(jax.ShapeDtyp...  110 us
    unnamed x5, local copies, waits for them, and re-layouts  6.3 us

profile of v1, /device:TPU:5, one launch (start us, length us, event | category | flops | bytes accessed | tf_op | source)
XLA Modules:
  0.0 117.4 jit_solution(5876400489729173128)
XLA Ops:
  0.6 110.4 %shard_map.94 = (bf16[256,512]{1,0:T(8,128)(2,1)}, f32[512,1024]{1,0:T(8,128)}, f32[1024,512]{1,0:T(8,128)}) custom-call(bf16[256,512]{1,0:T(8,128)(2,1)} %acts.1, bf16[256,512]{1,0:T(8,128)(2,1)} %cotangent.1, bf16[256,1024]{1,0:T(8,128)(2,1)} %pre_act.1, f32[512,1024]{1,0:T(8,128)} %up_store.1, f32[1,1024]{1,0:T(1,128)} %bitcast.3, ...), custom_call_target="tpu_custom_call" | custom-call | tf_op jit(solution)/shard_map/pallas_call | solution.py:305
  111.1 1.7 %copy.13 = bf16[256,512]{1,0:T(8,128)(2,1)} copy(bf16[256,512]{1,0:T(8,128)(2,1)} %get-tuple-element.6) | data formatting | bytes 524288
  112.8 0.0 copy-start
  112.8 3.3 %copy.14 = f32[512,1024]{1,0:T(8,128)} copy(f32[512,1024]{1,0:T(8,128)} %get-tuple-element.7) | data formatting | bytes 4194304
  116.1 0.0 copy-done
  116.1 1.3 %copy.15 = f32[1024,512]{1,0:T(8,128)} copy(f32[1024,512]{1,0:T(8,128)S(1)} %copy-done) | data formatting | bytes 4194304
Async XLA Ops:
  112.8 3.3 %copy-start = (f32[1024,512]{1,0:T(8,128)S(1)}, f32[1024,512]{1,0:T(8,128)}, u32[]{:S(2)}) copy-start(f32[1024,512]{1,0:T(8,128)} %get-tuple-element.8) | copy-start | bytes 6291460

commit v2 on v1

v2 whole, which is shorter than its diff:
```python
import functools
import math

import jax
import jax.numpy as jnp
from jax import lax
from jax.experimental import pallas as pl
from jax.experimental.pallas import tpu as pltpu
from jax.sharding import PartitionSpec as P

F32, BF16 = jnp.float32, jnp.bfloat16


def dot(left, right, dims):
    return lax.dot_general(left, right, (dims, ((), ())), preferred_element_type=F32)


def fitting(size, most):
    return most if size % most == 0 else size


def kernel(
    sizes,
    acts, cotangent, pre_act, up_store, up_scale, down_store, down_scale,
    grad_input, grad_up, grad_down,
    up_f32, down_f32,
    blocks, scaled_cols, acts_cols, act_group, dpre_group, down_bf, up_bf,
    pair_out, pair_in, far_out, far_in, d_act, gi_out, gi_in,
    gd_out, gd_in, gu_out, gu_in,
    load_sem,
    z_send, z_recv, col_send, col_recv, act_send, act_recv, dpre_send, dpre_recv,
    pair_send, pair_recv, far_send, far_recv, gi_send, gi_recv,
    gd_send, gd_recv, gu_send, gu_recv,
):
    reps, F, T = sizes
    n, d = acts.shape
    h = pre_act.shape[1]
    w = down_store.shape[1]
    half, sub = F // 2, F // T
    chunks, cw = blocks.shape[2], blocks.shape[4]
    per = w // cw
    parts, hp = dpre_group.shape[0], dpre_group.shape[2]
    norm_factor = 1.0 / math.sqrt(n * F * reps)
    r, f, z = lax.axis_index("rep"), lax.axis_index("fs"), lax.axis_index("tp")
    core, place = lax.rem(f, 2), lax.div(f, 2)
    partner = f + 1 - 2 * core
    mesh_ids = pl.DeviceIdType.MESH

    down_load = pltpu.make_async_copy(down_store, down_f32, load_sem.at[0])
    up_load = pltpu.make_async_copy(up_store, up_f32, load_sem.at[1])
    down_load.start()
    up_load.start()

    barrier = pltpu.get_barrier_semaphore()

    def greet(at, carry):
        to_f, to_z = lax.div(at, T), lax.rem(at, T)

        @pl.when((to_f != f) | (to_z != z))
        def _():
            pl.semaphore_signal(
                barrier, inc=1, device_id={"fs": to_f, "tp": to_z}, device_id_type=mesh_ids
            )

        return carry

    lax.fori_loop(0, F * T, greet, 0)
    for p in range(1, reps):
        pl.semaphore_signal(
            barrier, inc=1, device_id={"rep": lax.rem(r + p, reps)}, device_id_type=mesh_ids
        )

    def rows(at):
        return pl.ds(pl.multiple_of(at * n, n), n)

    def remote(src, dst, send, recv, where):
        return pltpu.make_async_remote_copy(
            src_ref=src, dst_ref=dst, send_sem=send, recv_sem=recv,
            device_id=where, device_id_type=mesh_ids,
        )

    def landed(ref, recv):
        remote(ref, ref, recv, recv, {"fs": partner}).wait_recv()

    def left_for(ref, send):
        remote(ref, ref, send, send, {"fs": partner}).wait_send()

    cols = (scaled_cols, acts_cols)

    def pass_on(a, block, g, way):
        @pl.when((z < T - 1) if way == 0 else (z > 0))
        def _():
            ref = blocks.at[a, block, g]
            to = z + 1 if way == 0 else z - 1
            remote(ref, ref, z_send.at[a, block, g, way], z_recv.at[a, block, g], {"tp": to}).start()

    def spread(a, block, g):
        target, q = block * sub + g // per, g % per

        @pl.when(target != f)
        def _():
            remote(
                blocks.at[a, block, g], cols[a].at[q, rows(f)],
                col_send.at[a, block, g], col_recv.at[a, f, q], {"fs": target},
            ).start()

        @pl.when(target == f)
        def _():
            cols[a][q, rows(f), :] = blocks[a, block, g]

    def own_block(a):
        for g in range(chunks):
            pass_on(a, z, g, 0)
            pass_on(a, z, g, 1)
        for g in range(chunks):
            spread(a, z, g)

    def arriving(a, s):
        for g in range(chunks):
            @pl.when(z - s >= 0)
            def _():
                landed(blocks.at[a, z - s, g], z_recv.at[a, z - s, g])
                pass_on(a, z - s, g, 0)
                spread(a, z - s, g)

            @pl.when(z + s <= T - 1)
            def _():
                landed(blocks.at[a, z + s, g], z_recv.at[a, z + s, g])
                pass_on(a, z + s, g, 1)
                spread(a, z + s, g)

    def cols_landed(a, source):
        @pl.when(source != f)
        def _():
            for q in range(per):
                landed(cols[a].at[q, rows(source)], col_recv.at[a, source, q])

    def group_start(group, send, recv):
        ref = group.at[rows(f)]
        for k in range(1, half):
            to = lax.rem(f + 2 * k, F)
            remote(ref, ref, send.at[k], recv.at[f], {"fs": to}).start()
        remote(ref, ref, send.at[0], recv.at[f], {"fs": partner}).start()

    def group_forward(group, send, recv):
        for k in range(1, half):
            source = lax.rem(f - 2 * k + F, F)
            ref = group.at[rows(source)]
            landed(ref, recv.at[source])
            remote(ref, ref, send.at[half - 1 + k], recv.at[source], {"fs": partner}).start()

    def forwards_landed(group, recv):
        for k in range(1, half):
            source = lax.rem(partner + 2 * k, F)
            landed(group.at[rows(source)], recv.at[source])

    def group_sent(group, send):
        for k in range(F - 1):
            left_for(group.at[rows(f)], send.at[k])

    scale = down_scale[:, pl.ds(pl.multiple_of(z * d, d), d)]
    scaled = (cotangent[...].astype(F32) * scale).astype(BF16)
    for g in range(chunks):
        blocks[0, z, g] = scaled[:, g * cw:(g + 1) * cw]
    positive = jnp.maximum(pre_act[...].astype(F32), 0.0)
    act_group[rows(f), :] = (positive * positive).astype(BF16)
    pl.semaphore_wait(barrier, F * T - 1 + reps - 1)
    own_block(0)
    group_start(act_group, act_send, act_recv)
    for g in range(chunks):
        blocks[1, z, g] = acts[:, g * cw:(g + 1) * cw]
    down_load.wait()
    down_bf[...] = down_f32[...].astype(BF16)
    for s in range(1, T):
        if s == T - 1:
            group_forward(act_group, act_send, act_recv)
        arriving(0, s)
    own_block(1)

    def partial_of(target, e):
        value = jnp.zeros((n, hp), F32)
        for q in range(per):
            value = value + dot(
                scaled_cols[q, rows(target), :],
                down_bf[e * hp:(e + 1) * hp, q * cw:(q + 1) * cw], ((1,), (1,)),
            )
        return value

    for e in range(parts):
        def for_partner(k, carry):
            i = lax.rem(place + k, half)
            if e == 0:
                cols_landed(0, 2 * i + 1 - core)
            pair_out[e, i] = partial_of(2 * i + 1 - core, e).astype(BF16)
            remote(
                pair_out.at[e, i], pair_in.at[e, i], pair_send.at[e, i], pair_recv.at[e, i],
                {"fs": partner},
            ).start()
            return carry

        lax.fori_loop(1, half + 1, for_partner, 0)
    for e in range(parts):
        def for_far(k, carry):
            i = lax.rem(place + k, half)
            if e == 0:
                cols_landed(0, 2 * i + core)
            value = partial_of(2 * i + core, e)
            landed(pair_in.at[e, i], pair_recv.at[e, i])
            far_out[e, i] = (value + pair_in[e, i].astype(F32)).astype(BF16)
            remote(
                far_out.at[e, i], far_in.at[e, place], far_send.at[e, i], far_recv.at[e, place],
                {"fs": 2 * i + core},
            ).start()
            return carry

        lax.fori_loop(1, half, for_far, 0)
    for e in range(parts):
        value = partial_of(f, e)
        landed(pair_in.at[e, place], pair_recv.at[e, place])
        d_act[e] = value + pair_in[e, place].astype(F32)

    landed(act_group.at[rows(partner)], act_recv.at[partner])
    forwards_landed(act_group, act_recv)
    gd_rows = gd_out.shape[1]

    def rep_copy(out, into, send, recv, c, p):
        to = lax.rem(r + p, reps)
        return remote(
            out.at[c], into.at[p - 1, c], send.at[p - 1, c], recv.at[p - 1, c], {"rep": to}
        )

    def down_step(c, carry):
        at = pl.ds(pl.multiple_of(c * gd_rows, gd_rows), gd_rows)
        for q in range(per):
            value = dot(act_group[:, at], scaled_cols[q], ((0,), (0,))) * norm_factor
            gd_out[c, :, q * cw:(q + 1) * cw] = value.astype(BF16)
        for p in range(1, reps):
            rep_copy(gd_out, gd_in, gd_send, gd_recv, c, p).start()
        return carry

    lax.fori_loop(0, gd_out.shape[0], down_step, 0)
    arriving(1, 1)
    for e in range(parts):
        total = d_act[e]
        for k in range(1, half):
            j = lax.rem(place + k, half)
            landed(far_in.at[e, j], far_recv.at[e, j])
            total = total + far_in[e, j].astype(F32)
        at = slice(e * hp, (e + 1) * hp)
        positive = jnp.maximum(pre_act[:, at].astype(F32), 0.0)
        dpre_group[e, rows(f), :] = (2.0 * positive * total * up_scale[:, at]).astype(BF16)
        group_start(dpre_group.at[e], dpre_send.at[e], dpre_recv.at[e])
        if e == 0:
            up_load.wait()
            up_bf[...] = up_f32[...].astype(BF16)
            for s in range(2, T - 1):
                arriving(1, s)
    if T > 2:
        arriving(1, T - 1)

    home = lax.div(f, sub)
    slot = z * sub + lax.rem(f, sub)

    def input_part(source):
        value = jnp.zeros((n, w), F32)
        for e in range(parts):
            value = value + dot(
                dpre_group[e, rows(source), :], up_bf[:, e * hp:(e + 1) * hp], ((1,), (1,))
            )
        gi_out[source] = value.astype(BF16)

        @pl.when((source != f) | (home != z))
        def _():
            remote(
                gi_out.at[source], gi_in.at[slot], gi_send.at[source], gi_recv.at[slot],
                {"fs": source, "tp": home},
            ).start()

        @pl.when((source == f) & (home == z))
        def _():
            gi_in[slot] = gi_out[source]

    input_part(f)
    for e in range(parts):
        group_forward(dpre_group.at[e], dpre_send.at[e], dpre_recv.at[e])
        landed(dpre_group.at[e, rows(partner)], dpre_recv.at[e, partner])
        forwards_landed(dpre_group.at[e], dpre_recv.at[e])
        if e == 0:
            for source in range(F):
                cols_landed(1, source)
        for q in range(per):
            value = dot(acts_cols[q], dpre_group[e], ((0,), (0,)))
            gu_out[e, q * cw:(q + 1) * cw, :] = (value * norm_factor).astype(BF16)
        for p in range(1, reps):
            rep_copy(gu_out, gu_in, gu_send, gu_recv, e, p).start()
    for k in range(1, half):
        input_part(lax.rem(f + 2 * k, F))
        input_part(lax.rem(partner + 2 * k, F))
    input_part(partner)

    def total_of(out, into, send, recv, c):
        for p in range(1, reps):
            rep_copy(out, into, send, recv, c, p).wait()
        value = out[c].astype(F32)
        for p in range(1, reps):
            value = value + into[p - 1, c].astype(F32)
        return value

    def finish_down(c, carry):
        at = pl.ds(pl.multiple_of(c * gd_rows, gd_rows), gd_rows)
        grad_down[at, :] = total_of(gd_out, gd_in, gd_send, gd_recv, c)
        return carry

    lax.fori_loop(0, gd_out.shape[0], finish_down, 0)
    for e in range(parts - 1):
        grad_up[:, e * hp:(e + 1) * hp] = total_of(gu_out, gu_in, gu_send, gu_recv, e)
    for j in range(sub):
        value = jnp.zeros((n, w), F32)
        for s in range(T):
            at = s * sub + j

            @pl.when((s != z) | (z * sub + j != f))
            def _():
                landed(gi_in.at[at], gi_recv.at[at])

            value = value + gi_in[at].astype(F32)
        grad_input[:, j * w:(j + 1) * w] = value.astype(BF16)
    grad_up[:, (parts - 1) * hp:] = total_of(gu_out, gu_in, gu_send, gu_recv, parts - 1)

    for a in range(2):
        for block in range(T):
            for g in range(chunks):
                @pl.when((block <= z) & (z < T - 1))
                def _():
                    left_for(blocks.at[a, block, g], z_send.at[a, block, g, 0])

                @pl.when((block >= z) & (z > 0))
                def _():
                    left_for(blocks.at[a, block, g], z_send.at[a, block, g, 1])

                @pl.when(block * sub + g // per != f)
                def _():
                    left_for(blocks.at[a, block, g], col_send.at[a, block, g])
    group_sent(act_group, act_send)
    for e in range(parts):
        group_sent(dpre_group.at[e], dpre_send.at[e])
        for i in range(half):
            left_for(pair_out.at[e, i], pair_send.at[e, i])

            @pl.when(i != place)
            def _():
                left_for(far_out.at[e, i], far_send.at[e, i])
    for source in range(F):
        @pl.when((source != f) | (home != z))
        def _():
            left_for(gi_out.at[source], gi_send.at[source])


def body(sizes, acts, cotangent, pre_act, up_store, up_scale, down_store, down_scale):
    reps, F, T = sizes
    n, d = acts.shape
    h = pre_act.shape[1]
    w = down_store.shape[1]
    half = F // 2
    cw = w // 2 if w % 256 == 0 else w
    per, chunks = w // cw, d // cw
    parts = 2 if h % 256 == 0 else 1
    hp = h // parts
    gd_rows = fitting(h, 256)
    gd_steps = h // gd_rows
    others = max(reps - 1, 1)
    sem = pltpu.SemaphoreType.DMA
    vmem, anywhere = (pl.BlockSpec(memory_space=s) for s in (pltpu.VMEM, pltpu.HBM))
    arrays = [
        ((w, h), F32), ((h, w), F32),
        ((2, T, chunks, n, cw), BF16),
        ((per, F * n, cw), BF16), ((per, F * n, cw), BF16),
        ((F * n, h), BF16), ((parts, F * n, hp), BF16),
        ((h, w), BF16), ((w, h), BF16),
        ((parts, half, n, hp), BF16), ((parts, half, n, hp), BF16),
        ((parts, half, n, hp), BF16), ((parts, half, n, hp), BF16),
        ((parts, n, hp), F32),
        ((F, n, w), BF16), ((F, n, w), BF16),
        ((gd_steps, gd_rows, w), BF16), ((others, gd_steps, gd_rows, w), BF16),
        ((parts, w, hp), BF16), ((others, parts, w, hp), BF16),
    ]
    held = sum(math.prod(shape) * jnp.dtype(kind).itemsize for shape, kind in arrays)
    held += 2 * w * h * 4 + 2 * (3 * n * d + n * h)
    return pl.pallas_call(
        functools.partial(kernel, sizes),
        out_shape=(
            jax.ShapeDtypeStruct((n, d), BF16),
            jax.ShapeDtypeStruct((w, h), F32),
            jax.ShapeDtypeStruct((h, w), F32),
        ),
        in_specs=[vmem, vmem, vmem, anywhere, vmem, anywhere, vmem],
        out_specs=(vmem, vmem, vmem),
        scratch_shapes=[pltpu.VMEM(shape, kind) for shape, kind in arrays] + [
            sem((2,)),
            sem((2, T, chunks, 2)), sem((2, T, chunks)), sem((2, T, chunks)), sem((2, F, per)),
            sem((F,)), sem((F,)), sem((parts, F)), sem((parts, F)),
            sem((parts, half)), sem((parts, half)), sem((parts, half)), sem((parts, half)),
            sem((F,)), sem((F,)),
            sem((others, gd_steps)), sem((others, gd_steps)),
            sem((others, parts)), sem((others, parts)),
        ],
        compiler_params=pltpu.CompilerParams(
            collective_id=0, has_side_effects=True,
            vmem_limit_bytes=min(held + 10 * 1024 * 1024, 60 * 1024 * 1024),
        ),
    )(
        acts, cotangent, pre_act, up_store, up_scale.reshape(1, h), down_store,
        down_scale.reshape(1, d * T),
    )


def solution(mesh):
    sizes = (mesh.shape["rep"], mesh.shape["fs"], mesh.shape["tp"])
    return jax.shard_map(
        functools.partial(body, sizes),
        mesh=mesh,
        in_specs=(
            P(("rep", "fs"), "tp"),
            P(("rep", "fs"), "tp"),
            P(("rep", "fs"), "tp"),
            P("fs", "tp"),
            P("tp"),
            P("tp", "fs"),
            P(),
        ),
        out_specs=(P(("rep", "fs"), "tp"), P("fs", "tp"), P("tp", "fs")),
        check_vma=False,
    )
```

time: 118 us -> 118 us (level)
  the two profiles are of different devices: /device:TPU:5 before, /device:TPU:1 now
where the time goes in v2:
time: 118 us
  Pallas kernels  106 us (90%)
  local copies, waits for them, and re-layouts  10.8 us (9%)
    pallas_call x1, Pallas kernels, body(): pl.pallas_call(functools.partial(kernel, sizes), out_shape=(jax.ShapeDtyp...  106 us
    unnamed x17, local copies, waits for them, and re-layouts  10.8 us

profile of v2, /device:TPU:1, one launch (start us, length us, event | category | flops | bytes accessed | tf_op | source)
XLA Modules:
  0.0 117.9 jit_solution(1241261720784978544)
XLA Ops:
  0.6 0.0 copy-start
  0.6 1.6 %copy-done = f32[512,1024]{1,0:T(8,128)S(1)} copy-done((f32[512,1024]{1,0:T(8,128)S(1)}, f32[512,1024]{1,0:T(8,128)}, u32[]{:S(2)}) %copy-start) | copy-done | bytes 2097176
  2.2 0.0 copy-start.1
  2.2 1.6 %copy-done.1 = f32[1024,512]{1,0:T(8,128)S(1)} copy-done((f32[1024,512]{1,0:T(8,128)S(1)}, f32[1024,512]{1,0:T(8,128)}, u32[]{:S(2)}) %copy-start.1) | copy-done | bytes 2097176
  3.8 0.0 copy-start.2
  3.8 1.0 copy-done.2
  4.9 0.0 copy-start.3
  4.9 0.9 copy-done.3
  5.8 0.0 copy-start.4
  5.8 0.9 copy-done.4
  6.8 0.0 copy-start.5
  6.8 0.7 copy-done.5
  7.5 0.0 copy-start.6
  7.5 0.7 copy-done.6
  8.1 106.4 %shard_map.94 = (bf16[256,512]{1,0:T(8,128)(2,1)S(1)}, f32[512,1024]{1,0:T(8,128)S(1)}, f32[1024,512]{1,0:T(8,128)S(1)}) custom-call(bf16[256,512]{1,0:T(8,128)(2,1)S(1)} %copy-done.3, bf16[256,512]{1,0:T(8,128)(2,1)S(1)} %copy-done.4, bf16[256,1024]{1,0:T(8,128)(2,1)S(1)} %copy-done.2, f32[512,1024]{1,0:T(8,128)S(1)} %copy-done, f32[1,1024]{1,0:T(1,128)S(1)} %bitcast.3, ...), custom_call_target="tpu_custom_call" | custom-call | tf_op jit(solution)/shard_map/pallas_call | solution.py:389
  114.5 0.7 copy.13
  115.2 1.3 %copy.14 = f32[512,1024]{1,0:T(8,128)} copy(f32[512,1024]{1,0:T(8,128)S(1)} %get-tuple-element.7) | data formatting | bytes 4194304
  116.5 1.3 %copy.15 = f32[1024,512]{1,0:T(8,128)} copy(f32[1024,512]{1,0:T(8,128)S(1)} %get-tuple-element.8) | data formatting | bytes 4194304
Async XLA Ops:
  0.6 1.6 %copy-start = (f32[512,1024]{1,0:T(8,128)S(1)}, f32[512,1024]{1,0:T(8,128)}, u32[]{:S(2)}) copy-start(f32[512,1024]{1,0:T(8,128)} %up_store.1) | copy-start | bytes 6291460
  2.2 1.6 %copy-start.1 = (f32[1024,512]{1,0:T(8,128)S(1)}, f32[1024,512]{1,0:T(8,128)}, u32[]{:S(2)}) copy-start(f32[1024,512]{1,0:T(8,128)} %down_store.1) | copy-start | bytes 6291460
  3.8 1.0 copy-start.2
  4.9 0.9 copy-start.3
  5.8 0.9 copy-start.4
  6.8 0.7 copy-start.5
  7.5 0.7 copy-start.6

commit v3 on v2

--- a/solution.py
+++ b/solution.py
@@ -25,11 +25,11 @@
     grad_input, grad_up, grad_down,
     up_f32, down_f32,
     blocks, scaled_cols, acts_cols, act_group, dpre_group, down_bf, up_bf,
-    pair_out, pair_in, far_out, far_in, d_act, gi_out, gi_in,
+    pair_out, pair_in, far_out, far_in, d_act, gi_out, gi_mid, gi_in,
     gd_out, gd_in, gu_out, gu_in,
     load_sem,
     z_send, z_recv, col_send, col_recv, act_send, act_recv, dpre_send, dpre_recv,
-    pair_send, pair_recv, far_send, far_recv, gi_send, gi_recv,
+    pair_send, pair_recv, far_send, far_recv, mid_send, mid_recv, gi_send, gi_recv,
     gd_send, gd_recv, gu_send, gu_recv,
 ):
     reps, F, T = sizes
@@ -258,8 +258,18 @@
     if T > 2:
         arriving(1, T - 1)
 
-    home = lax.div(f, sub)
-    slot = z * sub + lax.rem(f, sub)
+    def send_home(ref, source):
+        home, slot = lax.div(source, sub), z * sub + lax.rem(source, sub)
+
+        @pl.when(home != z)
+        def _():
+            remote(
+                ref, gi_in.at[slot], gi_send.at[source], gi_recv.at[slot], {"tp": home}
+            ).start()
+
+        @pl.when(home == z)
+        def _():
+            gi_in[slot] = ref[...]
 
     def input_part(source):
         value = jnp.zeros((n, w), F32)
@@ -269,34 +279,52 @@
             )
         gi_out[source] = value.astype(BF16)
 
-        @pl.when((source != f) | (home != z))
-        def _():
+        if source is f:
+            send_home(gi_out.at[source], f)
+        else:
             remote(
-                gi_out.at[source], gi_in.at[slot], gi_send.at[source], gi_recv.at[slot],
-                {"fs": source, "tp": home},
+                gi_out.at[source], gi_mid.at[f], mid_send.at[source], mid_recv.at[f],
+                {"fs": source},
             ).start()
 
-        @pl.when((source == f) & (home == z))
-        def _():
-            gi_in[slot] = gi_out[source]
+    def relay(source):
+        landed(gi_mid.at[source], mid_recv.at[source])
+        send_home(gi_mid.at[source], source)
 
     input_part(f)
     for e in range(parts):
-        group_forward(dpre_group.at[e], dpre_send.at[e], dpre_recv.at[e])
         landed(dpre_group.at[e, rows(partner)], dpre_recv.at[e, partner])
+    input_part(partner)
+    relay(partner)
+
+    def up_step(e):
         forwards_landed(dpre_group.at[e], dpre_recv.at[e])
-        if e == 0:
-            for source in range(F):
-                cols_landed(1, source)
         for q in range(per):
             value = dot(acts_cols[q], dpre_group[e], ((0,), (0,)))
             gu_out[e, q * cw:(q + 1) * cw, :] = (value * norm_factor).astype(BF16)
         for p in range(1, reps):
             rep_copy(gu_out, gu_in, gu_send, gu_recv, e, p).start()
+
+    for e in range(parts):
+        group_forward(dpre_group.at[e], dpre_send.at[e], dpre_recv.at[e])
+        if e == 0:
+            for source in range(F):
+                cols_landed(1, source)
+        if e < parts - 1:
+            up_step(e)
     for k in range(1, half):
         input_part(lax.rem(f + 2 * k, F))
+    forwards_landed(dpre_group.at[parts - 1], dpre_recv.at[parts - 1])
+    for k in range(1, half):
         input_part(lax.rem(partner + 2 * k, F))
-    input_part(partner)
+    for q in range(per):
+        value = dot(acts_cols[q], dpre_group[parts - 1], ((0,), (0,)))
+        gu_out[parts - 1, q * cw:(q + 1) * cw, :] = (value * norm_factor).astype(BF16)
+    for p in range(1, reps):
+        rep_copy(gu_out, gu_in, gu_send, gu_recv, parts - 1, p).start()
+    for k in range(1, half):
+        relay(lax.rem(f + 2 * k, F))
+        relay(lax.rem(partner + 2 * k, F))
 
     def total_of(out, into, send, recv, c):
         for p in range(1, reps):
@@ -319,7 +347,7 @@
         for s in range(T):
             at = s * sub + j
 
-            @pl.when((s != z) | (z * sub + j != f))
+            @pl.when(s != z)
             def _():
                 landed(gi_in.at[at], gi_recv.at[at])
 
@@ -351,9 +379,13 @@
             def _():
                 left_for(far_out.at[e, i], far_send.at[e, i])
     for source in range(F):
-        @pl.when((source != f) | (home != z))
-        def _():
-            left_for(gi_out.at[source], gi_send.at[source])
+        @pl.when(source != f)
+        def _():
+            left_for(gi_out.at[source], mid_send.at[source])
+
+        @pl.when(source // sub != z)
+        def _():
+            left_for(gi_mid.at[source], gi_send.at[source])
 
 
 def body(sizes, acts, cotangent, pre_act, up_store, up_scale, down_store, down_scale):
@@ -380,12 +412,10 @@
         ((parts, half, n, hp), BF16), ((parts, half, n, hp), BF16),
         ((parts, half, n, hp), BF16), ((parts, half, n, hp), BF16),
         ((parts, n, hp), F32),
-        ((F, n, w), BF16), ((F, n, w), BF16),
+        ((F, n, w), BF16), ((F, n, w), BF16), ((F, n, w), BF16),
         ((gd_steps, gd_rows, w), BF16), ((others, gd_steps, gd_rows, w), BF16),
         ((parts, w, hp), BF16), ((others, parts, w, hp), BF16),
     ]
-    held = sum(math.prod(shape) * jnp.dtype(kind).itemsize for shape, kind in arrays)
-    held += 2 * w * h * 4 + 2 * (3 * n * d + n * h)
     return pl.pallas_call(
         functools.partial(kernel, sizes),
         out_shape=(
@@ -400,13 +430,13 @@
             sem((2, T, chunks, 2)), sem((2, T, chunks)), sem((2, T, chunks)), sem((2, F, per)),
             sem((F,)), sem((F,)), sem((parts, F)), sem((parts, F)),
             sem((parts, half)), sem((parts, half)), sem((parts, half)), sem((parts, half)),
-            sem((F,)), sem((F,)),
+            sem((F,)), sem((F,)), sem((F,)), sem((F,)),
             sem((others, gd_steps)), sem((others, gd_steps)),
             sem((others, parts)), sem((others, parts)),
         ],
         compiler_params=pltpu.CompilerParams(
             collective_id=0, has_side_effects=True,
-            vmem_limit_bytes=min(held + 10 * 1024 * 1024, 60 * 1024 * 1024),
+            vmem_limit_bytes=60 * 1024 * 1024,
         ),
     )(
         acts, cotangent, pre_act, up_store, up_scale.reshape(1, h), down_store,

time: 118 us -> 105 us (0.89)
  the two profiles are of different devices: /device:TPU:1 before, /device:TPU:5 now
where the time goes in v3:
time: 105 us; the launch traced here: 104 us
  Pallas kernels  96.8 us (92%)
  local copies, waits for them, and re-layouts  6.3 us (6%)
    pallas_call x1, Pallas kernels, body(): pl.pallas_call(functools.partial(kernel, sizes), out_shape=(jax.ShapeDtyp...  96.8 us
    unnamed x5, local copies, waits for them, and re-layouts  6.3 us

profile of v3, /device:TPU:5, one launch (start us, length us, event | category | flops | bytes accessed | tf_op | source)
XLA Modules:
  0.0 103.8 jit_solution(5696279067631637642)
XLA Ops:
  0.6 96.8 %shard_map.94 = (bf16[256,512]{1,0:T(8,128)(2,1)}, f32[512,1024]{1,0:T(8,128)}, f32[1024,512]{1,0:T(8,128)}) custom-call(bf16[256,512]{1,0:T(8,128)(2,1)} %acts.1, bf16[256,512]{1,0:T(8,128)(2,1)} %cotangent.1, bf16[256,1024]{1,0:T(8,128)(2,1)} %pre_act.1, f32[512,1024]{1,0:T(8,128)} %up_store.1, f32[1,1024]{1,0:T(1,128)} %bitcast.3, ...), custom_call_target="tpu_custom_call" | custom-call | tf_op jit(solution)/shard_map/pallas_call | solution.py:419
  97.5 1.7 %copy.13 = bf16[256,512]{1,0:T(8,128)(2,1)} copy(bf16[256,512]{1,0:T(8,128)(2,1)} %get-tuple-element.6) | data formatting | bytes 524288
  99.1 0.0 copy-start
  99.1 3.3 %copy.14 = f32[512,1024]{1,0:T(8,128)} copy(f32[512,1024]{1,0:T(8,128)} %get-tuple-element.7) | data formatting | bytes 4194304
  102.5 0.0 copy-done
  102.5 1.3 %copy.15 = f32[1024,512]{1,0:T(8,128)} copy(f32[1024,512]{1,0:T(8,128)S(1)} %copy-done) | data formatting | bytes 4194304
Async XLA Ops:
  99.1 3.3 %copy-start = (f32[1024,512]{1,0:T(8,128)S(1)}, f32[1024,512]{1,0:T(8,128)}, u32[]{:S(2)}) copy-start(f32[1024,512]{1,0:T(8,128)} %get-tuple-element.8) | copy-start | bytes 6291460
